TPU v7x, 32 devices: a whole 2x2x4 slice. The times are simulated.
32 devices in a mesh: grp: 2 (over x), ep: 16 (over z, y, core).
Axes of the slice: x: 2, y: 2, z: 4, core: 2. Of those that a mesh axis runs over, the one named last changes fastest.
Arguments:
- tokens: bfloat16 [128, 2048], P(('grp', 'ep')), parts along dimension 0, may hold values from -30 to 30
- state: float32 [128, 16, 128, 128], P(('grp', 'ep')), parts along dimension 0, may hold values from -6 to 6
- route_ids: int32 [128, 2], P(('grp', 'ep')), parts along dimension 0, may hold values from 0 to 3, all different within a row; in each aligned block of 4 rows (0 to 3, 4 to 7, ...) at most 3 rows name the same one
- route_weights: bfloat16 [128, 2], P(('grp', 'ep')), parts along dimension 0, may hold values from 0.099609375 to 1
- norm_mix: float32 [2048], replicated, may hold values from 0.1 to 1.9
- w_query: bfloat16 [2048, 2048], P(None, 'ep'), may hold values from -0.125 to 0.125
- w_forget: bfloat16 [2048, 2048], P(None, 'ep'), may hold values from -0.125 to 0.125
- w_input: bfloat16 [2048, 2048], P(None, 'ep'), may hold values from -0.125 to 0.125
- w_gate: bfloat16 [2048, 2048], P(None, 'ep'), may hold values from -0.125 to 0.125
- lower_bound: float32 [2048], replicated, may hold values from 0.05 to 0.9
- head_gain: float32 [128], replicated, may hold values from 0.1 to 1.9
- w_out: bfloat16 [2048, 2048], P(None, 'ep'), may hold values from -0.125 to 0.125
- norm_ffn: float32 [2048], replicated, may hold values from 0.1 to 1.9
- expert_gate: bfloat16 [2048, 28672], P(None, 'ep'), may hold values from -0.125 to 0.125
- expert_up: bfloat16 [2048, 28672], P(None, 'ep'), may hold values from -0.125 to 0.125
- expert_down: bfloat16 [28672, 2048], P('ep'), may hold values from -0.0625 to 0.0625
Outputs:
- layer_out: bfloat16 [128, 2048], P(('grp', 'ep')), parts along dimension 0
- new_state: float32 [128, 16, 128, 128], P(('grp', 'ep')), parts along dimension 0
There are 2 independent parts, one for each index of `grp`. A program takes and returns all parts, laid end to end along the dimension named above; an argument that names none is the same for every part. Nothing has to cross between parts.
Inputs may be any that keep to these rules, and one draw needn't show every extreme that they name: `route_ids`: each row names 2 different experts; the rows of one device name no expert more than 3 times, and some device names one exactly 3 times.
All inputs are finite; a program needn't handle non-finite values.
Results may differ from a plain program's by a relative error of at most 0.008.
Values may be sent and summed in bfloat16 or wider, within the bound.
A program may use at most 64 MiB of HBM per device.

v0:
```python
import functools

import jax
import jax.numpy as jnp
from jax import lax
from jax.experimental import pallas as pl
from jax.experimental.pallas import tpu as pltpu
from jax.sharding import PartitionSpec as P

FF = 7168
EXPERTS = 4
VMEM = 67043328

epsilon = 1e-06
F32 = jnp.float32
BF16 = jnp.bfloat16


def rms_scale(values, gain):
    return values * lax.rsqrt(jnp.mean(values * values, axis=-1, keepdims=True) + epsilon) * gain


def kernel(
    n,
    tokens,
    state,
    ids,
    weights,
    norm_mix_in,
    w_query,
    w_forget,
    w_input,
    w_gate,
    lower_bound_in,
    head_gain_in,
    w_out,
    norm_ffn_in,
    expert_gate,
    expert_up,
    expert_down,
    layer_out,
    st,
    tok_buf,
    norm_mix,
    lower_bound,
    head_gain,
    norm_ffn,
    wp,
    wo,
    wg,
    wu,
    wd,
    xn,
    pj_send,
    pj_buf,
    gates,
    reads,
    mx_buf,
    col_buf,
    mid_buf,
    hid,
    ps,
    fw,
    summed,
    ret_buf,
    load_sem,
    send_sem,
    recv_sem,
):
    me = lax.axis_index("ep")
    rows, width = tokens.shape
    heads, dim = state.shape[1], state.shape[2]
    cols = w_query.shape[1]
    total = n * rows
    hidden = expert_gate.shape[1]
    group = n // EXPERTS // 2
    chunk = 16
    per = chunk // rows

    loads = [pltpu.make_async_copy(tokens, tok_buf.at[me], load_sem.at[0])]
    for j, w in enumerate((w_query, w_forget, w_input, w_gate)):
        loads.append(pltpu.make_async_copy(w, wp.at[j], load_sem.at[1 + j]))
    loads.append(pltpu.make_async_copy(state, st, load_sem.at[5]))
    loads.append(pltpu.make_async_copy(w_out, wo, load_sem.at[6]))
    loads.append(pltpu.make_async_copy(expert_gate, wg, load_sem.at[7]))
    loads.append(pltpu.make_async_copy(expert_up, wu, load_sem.at[8]))
    loads.append(pltpu.make_async_copy(expert_down, wd, load_sem.at[9]))
    small = [
        pltpu.make_async_copy(a, b, load_sem.at[10 + j])
        for j, (a, b) in enumerate(
            (
                (norm_mix_in, norm_mix),
                (lower_bound_in, lower_bound),
                (head_gain_in, head_gain),
                (norm_ffn_in, norm_ffn),
            )
        )
    ]

    core = lax.rem(me, 2)
    chip = me // 2
    chips = n // 2
    partner = me + 1 - 2 * core
    others = []
    for k in range(1, chips // 2 + 1):
        others.extend(sorted({k, chips - k}))

    def away(k):
        return lax.rem(me + 2 * k, n)

    barrier = pltpu.get_barrier_semaphore()
    for k in range(1, n):
        pl.semaphore_signal(
            barrier,
            inc=1,
            device_id={"ep": lax.rem(me + k, n)},
            device_id_type=pl.DeviceIdType.MESH,
        )
    for load in loads[:1] + small + loads[1:]:
        load.start()
    pl.semaphore_wait(barrier, n - 1)
    sent = []

    def send(phase, slot, source, target, peer):
        copy = pltpu.make_async_remote_copy(
            src_ref=source,
            dst_ref=target,
            send_sem=send_sem.at[phase, slot],
            recv_sem=recv_sem.at[phase, slot],
            device_id={"ep": peer},
            device_id_type=pl.DeviceIdType.MESH,
        )
        copy.start()
        sent.append(copy)
        return copy

    def spread(phase, buf):
        block = buf.at[me]
        direct = {k: send(phase, k, block, block, away(k)) for k in others}
        passed = [send(phase, chips, block, block, partner)]
        return direct, passed

    def pass_on(phase, buf, copies):
        direct, passed = copies
        for k in others:
            direct[k].wait_recv()
            block = buf.at[lax.rem(me - 2 * k + n, n)]
            passed.append(send(phase, chips + k, block, block, partner))
        for copy in passed:
            copy.wait_recv()

    loads[0].wait()
    copies = spread(0, tok_buf)
    for load in small:
        load.wait()
    pass_on(0, tok_buf, copies)

    def norm_chunk(c, carry):
        x = jnp.concatenate([tok_buf[c * per + i].astype(F32) for i in range(per)], axis=0)
        r0 = pl.multiple_of(c * chunk, chunk)
        xn[pl.ds(r0, chunk), :] = rms_scale(x, norm_mix[...]).astype(BF16)
        return carry

    lax.fori_loop(0, total // chunk, norm_chunk, 0, unroll=2)

    for load in loads[1:5]:
        load.wait()
    w_all = jnp.concatenate([wp[j] for j in range(4)], axis=1)
    acc = jnp.dot(xn[...], w_all, preferred_element_type=F32)
    for s in range(n):
        pj_send[s] = acc[s * rows : (s + 1) * rows, :].astype(BF16)
    copies = [
        send(1, k, pj_send.at[lax.rem(me + k, n)], pj_buf.at[me], lax.rem(me + k, n))
        for k in sorted(range(1, n), key=lambda k: min(k, n - k))
    ]
    pj_buf[me] = pj_send[me]
    loads[5].wait()
    for copy in copies:
        copy.wait_recv()

    def owned(j):
        return jnp.concatenate(
            [pj_buf[s][:, j * cols : (j + 1) * cols].astype(F32) for s in range(n)], axis=1
        )

    bound = lower_bound[...]
    forget_raw = owned(1)
    query_raw = owned(0)
    decay = bound + (1.0 - bound) * jax.nn.sigmoid(forget_raw)
    key_vec = (1.0 - bound) * jax.nn.sigmoid(-forget_raw)
    query_vec = jax.nn.silu(query_raw) * dim ** (-0.5)
    input_raw = owned(2)
    read_vec = query_vec * decay
    for h in range(heads):
        part = slice(h * dim, (h + 1) * dim)
        gates[h] = jnp.concatenate(
            [read_vec[:, part], decay[:, part], key_vec[:, part], input_raw[:, part]], axis=0
        )

    def read_step(h, carry):
        turned = gates[h].T
        out = [
            jnp.sum(turned[:, t : t + 1] * st[t, h], axis=0, keepdims=True) for t in range(rows)
        ]
        reads[h] = jnp.concatenate(out, axis=0)
        return carry

    lax.fori_loop(0, heads, read_step, 0, unroll=4)

    def update_step(h, carry):
        flat = gates[h]
        turned = flat.T
        for t in range(rows):
            st[t, h] = (
                turned[:, rows + t : rows + t + 1] * st[t, h]
                + turned[:, 2 * rows + t : 2 * rows + t + 1]
                * flat[3 * rows + t : 3 * rows + t + 1, :]
            )
        return carry

    gate_raw = owned(3)
    query_key = query_vec * key_vec
    mixed = jnp.concatenate(
        [
            rms_scale(
                reads[h]
                + jnp.sum(query_key[:, h * dim : (h + 1) * dim], axis=1, keepdims=True)
                * input_raw[:, h * dim : (h + 1) * dim],
                head_gain[...],
            )
            * jax.nn.silu(gate_raw[:, h * dim : (h + 1) * dim])
            for h in range(heads)
        ],
        axis=1,
    )
    mx_buf[me] = mixed.astype(BF16)

    copies = spread(2, mx_buf)
    loads[6].wait()
    pass_on(2, mx_buf, copies)

    def mixed_chunk(c, carry):
        x = jnp.concatenate([mx_buf[c * per + i].astype(F32) for i in range(per)], axis=0)
        r0 = pl.multiple_of(c * chunk, chunk)
        xn[pl.ds(r0, chunk), :] = x.astype(BF16)
        return carry

    lax.fori_loop(0, total // chunk, mixed_chunk, 0, unroll=2)
    col_buf[me] = jnp.dot(xn[...], wo[...], preferred_element_type=F32).astype(BF16)

    copies = spread(3, col_buf)
    pass_on(3, col_buf, copies)

    def middle_chunk(c, carry):
        r0 = pl.multiple_of(c * chunk, chunk)
        x = jnp.concatenate([tok_buf[c * per + i].astype(F32) for i in range(per)], axis=0)
        y = jnp.concatenate(
            [col_buf[s, pl.ds(r0, chunk), :].astype(F32) for s in range(n)], axis=1
        )
        middle = x + y
        for i in range(per):
            mid_buf[c * per + i] = middle[i * rows : (i + 1) * rows, :]
        xn[pl.ds(r0, chunk), :] = rms_scale(middle, norm_ffn[...]).astype(BF16)
        return carry

    lax.fori_loop(0, total // chunk, middle_chunk, 0, unroll=2)

    loads[7].wait()
    loads[8].wait()
    tile = 256 if hidden % 256 == 0 else hidden

    def up_tile(j, carry):
        part = pl.ds(pl.multiple_of(j * tile, tile) if tile % 128 == 0 else 0, tile)
        g = jnp.dot(xn[...], wg[:, part], preferred_element_type=F32)
        u = jnp.dot(xn[...], wu[:, part], preferred_element_type=F32)
        hid[:, part] = (jax.nn.silu(g) * u).astype(BF16)
        return carry

    lax.fori_loop(0, hidden // tile, up_tile, 0)
    loads[9].wait()
    out_tile = 256
    pieces = 2
    piece = width // pieces

    def down_tile(j, carry):
        part = pl.ds(pl.multiple_of(j * out_tile, out_tile), out_tile)
        d = jnp.dot(hid[...], wd[:, part], preferred_element_type=F32)
        for s in range(n):
            ps[s % 2, s // 2, :, part] = d[s * rows : (s + 1) * rows, :].astype(BF16)
        return carry

    per_piece = piece // out_tile
    halves = []
    for p in range(pieces):
        lax.fori_loop(p * per_piece, (p + 1) * per_piece, down_tile, 0, unroll=2)
        part = pl.ds(p * piece, piece)
        halves.append(
            send(4, p, ps.at[1 - core, :, :, part], fw.at[:, :, part], partner)
        )
    returns = []
    for p in range(pieces):
        part = pl.ds(p * piece, piece)
        halves[p].wait_recv()
        for c in range(chips):
            summed[c, :, part] = (
                ps[core, c, :, part].astype(F32) + fw[c, :, part].astype(F32)
            ).astype(BF16)
        for k in others:
            to = lax.rem(chip + k, chips)
            returns.append(
                send(
                    5 + p,
                    k,
                    summed.at[to, :, part],
                    ret_buf.at[chip, :, part],
                    away(k),
                )
            )
        ret_buf[chip, :, part] = summed[chip, :, part]
    lax.fori_loop(0, heads, update_step, 0, unroll=2)
    for copy in returns:
        copy.wait_recv()
    result = mid_buf[me]
    diagonal = lax.broadcasted_iota(jnp.int32, (rows, rows), 0) == lax.broadcasted_iota(
        jnp.int32, (rows, rows), 1
    )
    for e in range(EXPERTS):
        flat_share = jnp.sum(
            jnp.where(ids[...] == e, weights[...].astype(F32), 0.0), axis=0, keepdims=True
        )
        share = jnp.sum(jnp.where(diagonal, flat_share, 0.0), axis=1, keepdims=True)
        rows_e = ret_buf[e * group].astype(F32)
        for s in range(1, group):
            rows_e = rows_e + ret_buf[e * group + s].astype(F32)
        result = result + share * rows_e
    layer_out[...] = result.astype(BF16)

    for copy in sent:
        copy.wait_send()


def local(n, *args):
    (
        tokens,
        state,
        ids,
        weights,
        norm_mix,
        w_query,
        w_forget,
        w_input,
        w_gate,
        lower_bound,
        head_gain,
        w_out,
        norm_ffn,
        expert_gate,
        expert_up,
        expert_down,
    ) = args
    rows, width = tokens.shape
    heads, dim = state.shape[1], state.shape[2]
    cols = w_query.shape[1]
    hidden = expert_gate.shape[1]
    total = n * rows
    any_spec = pl.BlockSpec(memory_space=pltpu.HBM)
    vmem = pl.BlockSpec(memory_space=pltpu.VMEM)
    return pl.pallas_call(
        functools.partial(kernel, n),
        out_shape=(
            pltpu.VMEM(tokens.shape, tokens.dtype),
            pltpu.VMEM(state.shape, state.dtype),
        ),
        in_specs=[any_spec, any_spec, vmem, vmem] + [any_spec] * 12,
        out_specs=(vmem, vmem),
        scratch_shapes=[
            pltpu.VMEM((n, rows, width), BF16),
            pltpu.VMEM((1, width), F32),
            pltpu.VMEM((1, width), F32),
            pltpu.VMEM((1, dim), F32),
            pltpu.VMEM((1, width), F32),
            pltpu.VMEM((4, width, cols), BF16),
            pltpu.VMEM((width, cols), BF16),
            pltpu.VMEM((width, hidden), BF16),
            pltpu.VMEM((width, hidden), BF16),
            pltpu.VMEM((hidden, width), BF16),
            pltpu.VMEM((total, width), BF16),
            pltpu.VMEM((n, rows, 4 * cols), BF16),
            pltpu.VMEM((n, rows, 4 * cols), BF16),
            pltpu.VMEM((heads, 4 * rows, dim), F32),
            pltpu.VMEM((heads, rows, dim), F32),
            pltpu.VMEM((n, rows, width), BF16),
            pltpu.VMEM((n, total, cols), BF16),
            pltpu.VMEM((n, rows, width), F32),
            pltpu.VMEM((total, hidden), BF16),
            pltpu.VMEM((2, n // 2, rows, width), BF16),
            pltpu.VMEM((n // 2, rows, width), BF16),
            pltpu.VMEM((n // 2, rows, width), BF16),
            pltpu.VMEM((n // 2, rows, width), BF16),
            pltpu.SemaphoreType.DMA((14,)),
            pltpu.SemaphoreType.DMA((7, n)),
            pltpu.SemaphoreType.DMA((7, n)),
        ],
        compiler_params=pltpu.CompilerParams(
            collective_id=0,
            has_side_effects=True,
            vmem_limit_bytes=VMEM - 4 * state.size - 64 * 1024,
        ),
    )(
        tokens,
        state,
        ids.T,
        weights.T,
        norm_mix[None],
        w_query,
        w_forget,
        w_input,
        w_gate,
        lower_bound[None],
        head_gain[None],
        w_out,
        norm_ffn[None],
        expert_gate,
        expert_up,
        expert_down,
    )


def solution(mesh):
    return jax.shard_map(
        functools.partial(local, mesh.shape["ep"]),
        mesh=mesh,
        in_specs=(
            P(("grp", "ep"), None),
            P(("grp", "ep"), None, None, None),
            P(("grp", "ep"), None),
            P(("grp", "ep"), None),
            P(),
            P(None, "ep"),
            P(None, "ep"),
            P(None, "ep"),
            P(None, "ep"),
            P(),
            P(),
            P(None, "ep"),
            P(),
            P(None, "ep"),
            P(None, "ep"),
            P("ep", None),
        ),
        out_specs=(P(("grp", "ep"), None), P(("grp", "ep"), None, None, None)),
        check_vma=False,
    )
```

profile of v0, /device:TPU:0, one launch (start us, length us, event | category | flops | bytes accessed | tf_op | source)
XLA Modules:
  0.0 46.9 jit_solution(7528200032893756216)
XLA Ops:
  0.6 43.6 %shard_map.167 = (bf16[4,2048]{1,0:T(4,128)(2,1)S(1)}, f32[4,16,128,128]{3,2,1,0:T(8,128)S(1)}) custom-call(bf16[4,2048]{1,0:T(4,128)(2,1)} %tokens.1, f32[4,16,128,128]{3,2,1,0:T(8,128)} %state.1, s32[2,4]{1,0:T(2,128)} %bitcast.9, bf16[2,4]{1,0:T(2,128)(2,1)} %bitcast.10, f32[1,2048]{1,0:T(1,128)} %bitcast.6, bf16[2048,128]{1,0:T(8,128)(2,1)} %w_query.1, ...), custom_call_target="tpu_custom_call" | custom-call | tf_op jit(solution)/shard_map/pallas_call | solution.py:368
  44.3 0.6 %copy.20 = bf16[4,2048]{1,0:T(4,128)(2,1)} copy(bf16[4,2048]{1,0:T(4,128)(2,1)S(1)} %get-tuple-element.2) | data formatting | bytes 32768
  44.9 2.0 %copy.21 = f32[4,16,128,128]{3,2,1,0:T(8,128)} copy(f32[4,16,128,128]{3,2,1,0:T(8,128)S(1)} %get-tuple-element.3) | data formatting | bytes 8388608
where the time goes:
time: 47.1 us; the launch traced here: 46.9 us
  Pallas kernels  43.6 us (93%)
  local copies, waits for them, and re-layouts  2.62 us (6%)
  between operations  0.65 us (1%)
    pallas_call x1, Pallas kernels, local(): pl.pallas_call(functools.partial(kernel, n), out_shape=(pltpu.VMEM(tokens...  43.6 us
    unnamed x2, local copies, waits for them, and re-layouts  2.62 us

commit v1 on v0

v1 whole, which is shorter than its diff:
```python
import functools

import jax
import jax.numpy as jnp
from jax import lax
from jax.experimental import pallas as pl
from jax.experimental.pallas import tpu as pltpu
from jax.sharding import PartitionSpec as P

FF = 7168
EXPERTS = 4
VMEM = 67043328

epsilon = 1e-06
F32 = jnp.float32
BF16 = jnp.bfloat16


def rms_scale(values, gain):
    return values * lax.rsqrt(jnp.mean(values * values, axis=-1, keepdims=True) + epsilon) * gain


def kernel(
    n,
    tokens,
    state,
    ids,
    weights,
    norm_mix_in,
    w_query,
    w_forget,
    w_input,
    w_gate,
    lower_bound_in,
    head_gain_in,
    w_out,
    norm_ffn_in,
    expert_gate,
    expert_up,
    expert_down,
    layer_out,
    st,
    tok_buf,
    norm_mix,
    lower_bound,
    head_gain,
    norm_ffn,
    wp,
    wo,
    wg,
    wu,
    wd,
    xn,
    pj_send,
    pj_buf,
    gates,
    mx_buf,
    col_buf,
    mid_buf,
    squares,
    acc_gate,
    acc_up,
    hid,
    ps,
    fw,
    summed,
    ret_buf,
    load_sem,
    send_sem,
    recv_sem,
):
    me = lax.axis_index("ep")
    rows, width = tokens.shape
    heads, dim = state.shape[1], state.shape[2]
    cols = w_query.shape[1]
    total = n * rows
    hidden = expert_gate.shape[1]
    group = n // EXPERTS // 2
    both = 2 * rows

    loads = [pltpu.make_async_copy(tokens, tok_buf.at[me], load_sem.at[0])]
    for j, w in enumerate((w_query, w_forget, w_input, w_gate)):
        loads.append(pltpu.make_async_copy(w, wp.at[j], load_sem.at[1 + j]))
    loads.append(pltpu.make_async_copy(state, st, load_sem.at[5]))
    loads.append(pltpu.make_async_copy(w_out, wo, load_sem.at[6]))
    loads.append(pltpu.make_async_copy(expert_gate, wg, load_sem.at[7]))
    loads.append(pltpu.make_async_copy(expert_up, wu, load_sem.at[8]))
    loads.append(pltpu.make_async_copy(expert_down, wd, load_sem.at[9]))
    small = [
        pltpu.make_async_copy(a, b, load_sem.at[10 + j])
        for j, (a, b) in enumerate(
            (
                (norm_mix_in, norm_mix),
                (lower_bound_in, lower_bound),
                (head_gain_in, head_gain),
                (norm_ffn_in, norm_ffn),
            )
        )
    ]

    core = lax.rem(me, 2)
    chip = me // 2
    chips = n // 2
    partner = me + 1 - 2 * core

    def flip(index, k):
        bit = 1
        while bit <= k:
            if k & bit:
                index = index + bit * (1 - 2 * lax.rem(index // bit, 2))
            bit *= 2
        return index

    at = [flip(chip, k) for k in range(chips)]
    same = [2 * at[k] + core for k in range(chips)]
    cross = [2 * at[k] + 1 - core for k in range(chips)]
    far_first = list(range(chips - 1, 0, -1))

    barrier = pltpu.get_barrier_semaphore()
    for k in far_first + [0]:
        for peer in (same[k], cross[k]) if k else (partner,):
            pl.semaphore_signal(
                barrier, inc=1, device_id={"ep": peer}, device_id_type=pl.DeviceIdType.MESH
            )
    for load in loads[:1] + small + loads[1:]:
        load.start()
    pl.semaphore_wait(barrier, n - 1)
    sent = []

    def send(phase, slot, source, target, peer):
        copy = pltpu.make_async_remote_copy(
            src_ref=source,
            dst_ref=target,
            send_sem=send_sem.at[phase, slot],
            recv_sem=recv_sem.at[phase, slot],
            device_id={"ep": peer},
            device_id_type=pl.DeviceIdType.MESH,
        )
        copy.start()
        sent.append(copy)
        return copy

    def spread(phase, buf):
        block = buf.at[me]
        direct = {k: send(phase, k, block, block, cross[k]) for k in far_first}
        return direct, {0: send(phase, 0, block, block, partner)}

    def forward(phase, buf, copies, ks):
        direct, passed = copies
        for k in ks:
            if k:
                direct[k].wait_recv()
                block = buf.at[cross[k]]
                passed[k] = send(phase, chips + k, block, block, partner)

    def arrive(copies, ks):
        for k in ks:
            copies[1][k].wait_recv()

    def batches(count):
        inner = [[i, i + 1] for i in range(1, count - 1, 2)]
        return [[0]] + inner + ([[count - 1]] if count > 1 else [])

    def chip_rows(buf, k):
        return [buf[2 * at[k] + c].astype(F32) for c in range(2)]

    loads[0].wait()
    copies = spread(0, tok_buf)
    for load in small:
        load.wait()
    pairs = [[2 * j, 2 * j + 1] for j in range(chips // 2)]

    def norm_pair(ks):
        x = jnp.concatenate([part for k in ks for part in chip_rows(tok_buf, k)], axis=0)
        for i, k in enumerate(ks):
            mid_buf[at[k]] = x[i * both : (i + 1) * both, :]
        xn[ks[0] * both : (ks[0] + 2) * both, :] = rms_scale(x, norm_mix[...]).astype(BF16)

    for j, ks in enumerate(pairs):
        forward(0, tok_buf, copies, ks)
        if j:
            arrive(copies, pairs[j - 1])
            norm_pair(pairs[j - 1])
    arrive(copies, pairs[-1])
    norm_pair(pairs[-1])

    for load in loads[1:5]:
        load.wait()
    w_all = jnp.concatenate([wp[j] for j in range(4)], axis=1)
    acc = jnp.dot(xn[...], w_all, preferred_element_type=F32)
    for s in range(n):
        pj_send[s] = acc[s * rows : (s + 1) * rows, :].astype(BF16)
    moved = {}
    for k in far_first + [0]:
        for r, peer in enumerate((same[k], cross[k])):
            if k or r:
                source = pj_send.at[2 * k + (core if r == 0 else 1 - core)]
                moved[k, r] = send(1, 2 * k + r, source, pj_buf.at[me], peer)
    pj_buf[me] = pj_send[core]

    per_head = max(1, dim // cols)
    head_chips = max(1, per_head // 2)
    chip_heads = head_chips * 2 * cols // dim
    loads[5].wait()

    def head_step(h, first):
        def owned(j):
            return jnp.concatenate(
                [
                    pj_buf[first + i][:, j * cols : (j + 1) * cols].astype(F32)
                    for i in range(per_head)
                ],
                axis=1,
            )

        bound = lower_bound[h]
        forget_raw = owned(1)
        decay = bound + (1.0 - bound) * jax.nn.sigmoid(forget_raw)
        key_vec = (1.0 - bound) * jax.nn.sigmoid(-forget_raw)
        query_vec = jax.nn.silu(owned(0)) * dim ** (-0.5)
        input_raw = owned(2)
        flat = jnp.concatenate([query_vec * decay, decay, key_vec, input_raw], axis=0)
        gates[h] = flat
        turned = flat.T
        out = [
            jnp.sum(turned[:, t : t + 1] * st[t, h], axis=0, keepdims=True) for t in range(rows)
        ]
        read = jnp.concatenate(out, axis=0) + input_raw * jnp.sum(
            query_vec * key_vec, axis=1, keepdims=True
        )
        mixed = rms_scale(read, head_gain[...]) * jax.nn.silu(owned(3))
        part = pl.ds(pl.multiple_of(h * dim, dim), dim)
        mx_buf[me, :, part] = mixed.astype(BF16)

    for batch in batches(chips // head_chips):
        for m in batch:
            for k in range(m * head_chips, (m + 1) * head_chips):
                for r in range(2):
                    if k or r:
                        moved[k, r].wait_recv()
        for m in batch:
            base = flip(chip // head_chips, m)
            for i in range(chip_heads):
                head_step(base * chip_heads + i, base * head_chips * 2 + i * per_head)

    def update_step(h, carry):
        flat = gates[h]
        turned = flat.T
        for t in range(rows):
            st[t, h] = (
                turned[:, rows + t : rows + t + 1] * st[t, h]
                + turned[:, 2 * rows + t : 2 * rows + t + 1]
                * flat[3 * rows + t : 3 * rows + t + 1, :]
            )
        return carry

    first_part = heads * 5 // 8
    second_part = heads * 7 // 8

    copies = spread(2, mx_buf)
    loads[6].wait()
    lax.fori_loop(0, first_part, update_step, 0, unroll=2)

    def gather_pair(ks):
        x = jnp.concatenate([part for k in ks for part in chip_rows(mx_buf, k)], axis=0)
        xn[ks[0] * both : (ks[0] + 2) * both, :] = x.astype(BF16)

    for j, ks in enumerate(pairs):
        forward(2, mx_buf, copies, ks)
        if j:
            arrive(copies, pairs[j - 1])
            gather_pair(pairs[j - 1])
    arrive(copies, pairs[-1])
    gather_pair(pairs[-1])

    acc = jnp.dot(xn[...], wo[...], preferred_element_type=F32)
    for k in range(chips):
        col_buf[me, at[k]] = acc[k * both : (k + 1) * both, :].astype(BF16)

    copies = spread(3, col_buf)
    lax.fori_loop(first_part, second_part, update_step, 0, unroll=2)
    loads[7].wait()
    loads[8].wait()
    tile = 256 if hidden % 256 == 0 else hidden
    slab_chips = max(1, 256 // (2 * cols))
    slab = slab_chips * 2 * cols
    slabs = chips // slab_chips
    plan = batches(slabs)

    def slab_of(m):
        base = flip(chip // slab_chips, m)
        first = base * slab_chips * 2
        part = pl.ds(pl.multiple_of(base * slab, slab), slab)
        y = jnp.concatenate(
            [col_buf[first + i].astype(F32) for i in range(2 * slab_chips)], axis=2
        )
        middle = mid_buf[:, :, part] + y
        mid_buf[:, :, part] = middle
        scaled = (middle * norm_ffn[:, part]).reshape(total, slab).astype(BF16)
        return part, scaled, jnp.sum((middle * middle).reshape(total, slab), axis=1, keepdims=True)

    def members(batch):
        return [k for m in batch for k in range(m * slab_chips, (m + 1) * slab_chips)]

    for b, batch in enumerate(plan):
        if b == 0:
            forward(3, col_buf, copies, members(batch))
        if b + 1 < len(plan) and b > 0:
            forward(3, col_buf, copies, members(plan[b + 1]))
        if b == 0 and len(plan) > 1:
            arrive(copies, members(batch))
        else:
            arrive(copies, members(batch))
        ready = [slab_of(m) for m in batch]
        power = sum(r[2] for r in ready)
        if b:
            power = power + squares[...]
        last = b + 1 == len(plan)
        if last:
            scale = lax.rsqrt(power / width + epsilon)
        else:
            squares[...] = power
        for j in range(hidden // tile):
            span = slice(j * tile, (j + 1) * tile)
            g = sum(jnp.dot(r[1], wg[r[0], span], preferred_element_type=F32) for r in ready)
            u = sum(jnp.dot(r[1], wu[r[0], span], preferred_element_type=F32) for r in ready)
            if b:
                g = g + acc_gate[:, span]
                u = u + acc_up[:, span]
            if last:
                hid[:, span] = (jax.nn.silu(g * scale) * (u * scale)).astype(BF16)
            else:
                acc_gate[:, span] = g
                acc_up[:, span] = u
        if b == 0 and len(plan) > 1:
            forward(3, col_buf, copies, members(plan[1]))

    loads[9].wait()
    out_tile = 256
    pieces = 4
    piece = width // pieces

    halves = []
    for p in range(pieces):
        for q in range(piece // out_tile):
            part = slice(p * piece + q * out_tile, p * piece + (q + 1) * out_tile)
            d = jnp.dot(hid[...], wd[:, part], preferred_element_type=F32)
            for s in range(n):
                ps[s % 2, s // 2, :, part] = d[s * rows : (s + 1) * rows, :].astype(BF16)
        part = pl.ds(p * piece, piece)
        halves.append(send(4, p, ps.at[core, :, :, part], fw.at[:, :, part], partner))
    returns = []
    for p in range(pieces):
        part = pl.ds(p * piece, piece)
        halves[p].wait_recv()
        for c in range(chips):
            summed[c, :, part] = (
                ps[1 - core, c, :, part].astype(F32) + fw[c, :, part].astype(F32)
            ).astype(BF16)
        for k in far_first + [0]:
            returns.append(
                send(
                    5 + p,
                    k,
                    summed.at[at[k], :, part],
                    ret_buf.at[chip, :, part],
                    cross[k],
                )
            )
    lax.fori_loop(second_part, heads, update_step, 0, unroll=2)
    for copy in returns:
        copy.wait_recv()
    own = mid_buf[chip]
    result = jnp.where(core == 0, own[:rows, :], own[rows:, :])
    diagonal = lax.broadcasted_iota(jnp.int32, (rows, rows), 0) == lax.broadcasted_iota(
        jnp.int32, (rows, rows), 1
    )
    for e in range(EXPERTS):
        flat_share = jnp.sum(
            jnp.where(ids[...] == e, weights[...].astype(F32), 0.0), axis=0, keepdims=True
        )
        share = jnp.sum(jnp.where(diagonal, flat_share, 0.0), axis=1, keepdims=True)
        rows_e = ret_buf[e * group].astype(F32)
        for s in range(1, group):
            rows_e = rows_e + ret_buf[e * group + s].astype(F32)
        result = result + share * rows_e
    layer_out[...] = result.astype(BF16)

    for copy in sent:
        copy.wait_send()


def local(n, *args):
    (
        tokens,
        state,
        ids,
        weights,
        norm_mix,
        w_query,
        w_forget,
        w_input,
        w_gate,
        lower_bound,
        head_gain,
        w_out,
        norm_ffn,
        expert_gate,
        expert_up,
        expert_down,
    ) = args
    rows, width = tokens.shape
    heads, dim = state.shape[1], state.shape[2]
    cols = w_query.shape[1]
    hidden = expert_gate.shape[1]
    total = n * rows
    any_spec = pl.BlockSpec(memory_space=pltpu.HBM)
    vmem = pl.BlockSpec(memory_space=pltpu.VMEM)
    return pl.pallas_call(
        functools.partial(kernel, n),
        out_shape=(
            pltpu.VMEM(tokens.shape, tokens.dtype),
            pltpu.VMEM(state.shape, state.dtype),
        ),
        in_specs=[any_spec, any_spec, vmem, vmem] + [any_spec] * 12,
        out_specs=(vmem, vmem),
        scratch_shapes=[
            pltpu.VMEM((n, rows, width), BF16),
            pltpu.VMEM((1, width), F32),
            pltpu.VMEM((heads, 1, dim), F32),
            pltpu.VMEM((1, dim), F32),
            pltpu.VMEM((1, width), F32),
            pltpu.VMEM((4, width, cols), BF16),
            pltpu.VMEM((width, cols), BF16),
            pltpu.VMEM((width, hidden), BF16),
            pltpu.VMEM((width, hidden), BF16),
            pltpu.VMEM((hidden, width), BF16),
            pltpu.VMEM((total, width), BF16),
            pltpu.VMEM((n, rows, 4 * cols), BF16),
            pltpu.VMEM((n, rows, 4 * cols), BF16),
            pltpu.VMEM((heads, 4 * rows, dim), F32),
            pltpu.VMEM((n, rows, width), BF16),
            pltpu.VMEM((n, n // 2, 2 * rows, cols), BF16),
            pltpu.VMEM((n // 2, 2 * rows, width), F32),
            pltpu.VMEM((total, 1), F32),
            pltpu.VMEM((total, hidden), F32),
            pltpu.VMEM((total, hidden), F32),
            pltpu.VMEM((total, hidden), BF16),
            pltpu.VMEM((2, n // 2, rows, width), BF16),
            pltpu.VMEM((n // 2, rows, width), BF16),
            pltpu.VMEM((n // 2, rows, width), BF16),
            pltpu.VMEM((n // 2, rows, width), BF16),
            pltpu.SemaphoreType.DMA((14,)),
            pltpu.SemaphoreType.DMA((9, n)),
            pltpu.SemaphoreType.DMA((9, n)),
        ],
        compiler_params=pltpu.CompilerParams(
            collective_id=0,
            has_side_effects=True,
            vmem_limit_bytes=VMEM - 4 * state.size - 64 * 1024,
        ),
    )(
        tokens,
        state,
        ids.T,
        weights.T,
        norm_mix[None],
        w_query,
        w_forget,
        w_input,
        w_gate,
        lower_bound.reshape(heads, 1, dim),
        head_gain[None],
        w_out,
        norm_ffn[None],
        expert_gate,
        expert_up,
        expert_down,
    )


def solution(mesh):
    return jax.shard_map(
        functools.partial(local, mesh.shape["ep"]),
        mesh=mesh,
        in_specs=(
            P(("grp", "ep"), None),
            P(("grp", "ep"), None, None, None),
            P(("grp", "ep"), None),
            P(("grp", "ep"), None),
            P(),
            P(None, "ep"),
            P(None, "ep"),
            P(None, "ep"),
            P(None, "ep"),
            P(),
            P(),
            P(None, "ep"),
            P(),
            P(None, "ep"),
            P(None, "ep"),
            P("ep", None),
        ),
        out_specs=(P(("grp", "ep"), None), P(("grp", "ep"), None, None, None)),
        check_vma=False,
    )
```

time: 47.1 us -> 46 us (0.977)
  Pallas kernels: 43.6 us -> 42.5 us
    pallas_call x1, Pallas kernels: 43.6 us -> 42.5 us  [local(): pl.pallas_call(functools.partial(kernel, n), out_shape=(pltpu.VMEM(tokens...]
where the time goes in v1:
time: 46 us; the launch traced here: 45.8 us
  Pallas kernels  42.5 us (92%)
  local copies, waits for them, and re-layouts  2.62 us (6%)
  between operations  0.65 us (1%)
    pallas_call x1, Pallas kernels, local(): pl.pallas_call(functools.partial(kernel, n), out_shape=(pltpu.VMEM(tokens...  42.5 us
    unnamed x2, local copies, waits for them, and re-layouts  2.62 us

profile of v1, /device:TPU:0, one launch (start us, length us, event | category | flops | bytes accessed | tf_op | source)
XLA Modules:
  0.0 45.8 jit_solution(14004930514747330156)
XLA Ops:
  0.6 42.5 %shard_map.167 = (bf16[4,2048]{1,0:T(4,128)(2,1)S(1)}, f32[4,16,128,128]{3,2,1,0:T(8,128)S(1)}) custom-call(bf16[4,2048]{1,0:T(4,128)(2,1)} %tokens.1, f32[4,16,128,128]{3,2,1,0:T(8,128)} %state.1, s32[2,4]{1,0:T(2,128)} %bitcast.9, bf16[2,4]{1,0:T(2,128)(2,1)} %bitcast.10, f32[1,2048]{1,0:T(1,128)} %bitcast.6, bf16[2048,128]{1,0:T(8,128)(2,1)} %w_query.1, ...), custom_call_target="tpu_custom_call" | custom-call | tf_op jit(solution)/shard_map/pallas_call | solution.py:419
  43.2 0.6 %copy.20 = bf16[4,2048]{1,0:T(4,128)(2,1)} copy(bf16[4,2048]{1,0:T(4,128)(2,1)S(1)} %get-tuple-element.2) | data formatting | bytes 32768
  43.8 2.0 %copy.21 = f32[4,16,128,128]{3,2,1,0:T(8,128)} copy(f32[4,16,128,128]{3,2,1,0:T(8,128)S(1)} %get-tuple-element.3) | data formatting | bytes 8388608

commit v2 on v1

--- a/solution.py
+++ b/solution.py
@@ -68,6 +68,7 @@
     load_sem,
     send_sem,
     recv_sem,
+    late_sem,
 ):
     me = lax.axis_index("ep")
     rows, width = tokens.shape
@@ -111,24 +112,50 @@
             bit *= 2
         return index
 
+    bits = [1 << b for b in range(chips.bit_length() - 1)]
     at = [flip(chip, k) for k in range(chips)]
     same = [2 * at[k] + core for k in range(chips)]
     cross = [2 * at[k] + 1 - core for k in range(chips)]
     far_first = list(range(chips - 1, 0, -1))
-
     barrier = pltpu.get_barrier_semaphore()
-    for k in far_first + [0]:
-        for peer in (same[k], cross[k]) if k else (partner,):
-            pl.semaphore_signal(
-                barrier, inc=1, device_id={"ep": peer}, device_id_type=pl.DeviceIdType.MESH
-            )
-    for load in loads[:1] + small + loads[1:]:
+    late = chip == chips - 1
+
+    def signal(semaphore, peer):
+        pl.semaphore_signal(
+            semaphore, inc=1, device_id={"ep": peer}, device_id_type=pl.DeviceIdType.MESH
+        )
+
+    @pl.when(late)
+    def _():
+        signal(barrier, partner)
+
+    @pl.when(jnp.logical_not(late))
+    def _():
+        for k in far_first:
+            signal(barrier, same[k])
+            signal(barrier, cross[k])
+        signal(barrier, partner)
+
+    loads[0].start()
+
+    @pl.when(late)
+    def _():
+        pl.semaphore_wait(barrier, n - 1)
+        for k in far_first:
+            signal(late_sem, same[k])
+            signal(late_sem, cross[k])
+
+    for load in small + loads[1:]:
         load.start()
-    pl.semaphore_wait(barrier, n - 1)
+
+    @pl.when(jnp.logical_not(late))
+    def _():
+        pl.semaphore_wait(barrier, n - 3)
+
     sent = []
 
-    def send(phase, slot, source, target, peer):
-        copy = pltpu.make_async_remote_copy(
+    def handle(phase, slot, source, target, peer):
+        return pltpu.make_async_remote_copy(
             src_ref=source,
             dst_ref=target,
             send_sem=send_sem.at[phase, slot],
@@ -136,36 +163,74 @@
             device_id={"ep": peer},
             device_id_type=pl.DeviceIdType.MESH,
         )
+
+    def send(phase, slot, source, target, peer):
+        copy = handle(phase, slot, source, target, peer)
         copy.start()
         sent.append(copy)
         return copy
 
-    def spread(phase, buf):
-        block = buf.at[me]
-        direct = {k: send(phase, k, block, block, cross[k]) for k in far_first}
-        return direct, {0: send(phase, 0, block, block, partner)}
-
-    def forward(phase, buf, copies, ks):
-        direct, passed = copies
+    def scatter(phase, block, near=0, order=None):
+        return {
+            k: (
+                [send(phase, k, block, block, cross[k])]
+                + ([send(phase, chips + k, block, block, same[k])] if k <= near else [])
+            )
+            for k in order or far_first
+        }
+
+    def forward(phase, buf, copies, passed, ks, near=0):
         for k in ks:
-            if k:
-                direct[k].wait_recv()
+            for part in copies:
+                if k:
+                    for copy in part[k]:
+                        copy.wait_recv()
+            if k == 0:
+                passed[k] = send(phase, 0, buf.at[me], buf.at[me], partner)
+            elif k > near:
                 block = buf.at[cross[k]]
                 passed[k] = send(phase, chips + k, block, block, partner)
 
-    def arrive(copies, ks):
+    def arrive(passed, ks):
         for k in ks:
-            copies[1][k].wait_recv()
-
-    def batches(count):
-        inner = [[i, i + 1] for i in range(1, count - 1, 2)]
-        return [[0]] + inner + ([[count - 1]] if count > 1 else [])
+            if k in passed:
+                passed[k].wait_recv()
+
+    shares = [(0, chips // 2), (chips // 2, chips * 3 // 4), (chips * 3 // 4, chips)]
+
+    def base_of(index, lo, hi):
+        return flip(index // (hi - lo), lo // (hi - lo)) * (hi - lo)
 
     def chip_rows(buf, k):
         return [buf[2 * at[k] + c].astype(F32) for c in range(2)]
-
     loads[0].wait()
-    copies = spread(0, tok_buf)
+    own = tok_buf.at[me]
+    to_late = sum(bit * (1 - lax.rem(chip // bit, 2)) for bit in bits)
+    direct = [handle(0, k, own, own, cross[k] if k else partner) for k in range(chips)]
+    extra = pltpu.make_async_remote_copy(
+        src_ref=own,
+        dst_ref=own,
+        send_sem=send_sem.at[7, 0],
+        recv_sem=recv_sem.at[0, chips + to_late],
+        device_id={"ep": n - 2 + core},
+        device_id_type=pl.DeviceIdType.MESH,
+    )
+    for k in far_first:
+
+        @pl.when(at[k] != chips - 1)
+        def _(k=k):
+            direct[k].start()
+
+    @pl.when(jnp.logical_not(late))
+    def _():
+        direct[0].start()
+        pl.semaphore_wait(late_sem, 2)
+        extra.start()
+
+    handle(0, to_late, own, own, n - 1 - core).start()
+    sent.extend(direct)
+    through = []
+
     for load in small:
         load.wait()
     pairs = [[2 * j, 2 * j + 1] for j in range(chips // 2)]
@@ -176,14 +241,27 @@
             mid_buf[at[k]] = x[i * both : (i + 1) * both, :]
         xn[ks[0] * both : (ks[0] + 2) * both, :] = rms_scale(x, norm_mix[...]).astype(BF16)
 
+    def pass_on(k):
+        direct[k].wait_recv()
+        block = tok_buf.at[cross[k]]
+        through.append(handle(0, chips + k, block, block, partner))
+
+        @pl.when(jnp.logical_not(late))
+        def _():
+            through[-1].start()
+
+    def settle_pair(ks):
+        for k in ks:
+            (through[k - 1] if k else direct[0]).wait_recv()
+        norm_pair(ks)
+
     for j, ks in enumerate(pairs):
-        forward(0, tok_buf, copies, ks)
+        for k in ks:
+            if k:
+                pass_on(k)
         if j:
-            arrive(copies, pairs[j - 1])
-            norm_pair(pairs[j - 1])
-    arrive(copies, pairs[-1])
-    norm_pair(pairs[-1])
-
+            settle_pair(pairs[j - 1])
+    settle_pair(pairs[-1])
     for load in loads[1:5]:
         load.wait()
     w_all = jnp.concatenate([wp[j] for j in range(4)], axis=1)
@@ -197,7 +275,6 @@
                 source = pj_send.at[2 * k + (core if r == 0 else 1 - core)]
                 moved[k, r] = send(1, 2 * k + r, source, pj_buf.at[me], peer)
     pj_buf[me] = pj_send[core]
-
     per_head = max(1, dim // cols)
     head_chips = max(1, per_head // 2)
     chip_heads = head_chips * 2 * cols // dim
@@ -219,29 +296,37 @@
         key_vec = (1.0 - bound) * jax.nn.sigmoid(-forget_raw)
         query_vec = jax.nn.silu(owned(0)) * dim ** (-0.5)
         input_raw = owned(2)
-        flat = jnp.concatenate([query_vec * decay, decay, key_vec, input_raw], axis=0)
-        gates[h] = flat
-        turned = flat.T
-        out = [
-            jnp.sum(turned[:, t : t + 1] * st[t, h], axis=0, keepdims=True) for t in range(rows)
-        ]
-        read = jnp.concatenate(out, axis=0) + input_raw * jnp.sum(
-            query_vec * key_vec, axis=1, keepdims=True
-        )
+        read_vec = query_vec * decay
+        gates[h] = jnp.concatenate([read_vec, decay, key_vec, input_raw], axis=0)
+        wide = jnp.dot(
+            read_vec,
+            jnp.concatenate([st[t, h] for t in range(rows)], axis=1),
+            preferred_element_type=F32,
+        )
+        read = jnp.concatenate(
+            [wide[t : t + 1, t * dim : (t + 1) * dim] for t in range(rows)], axis=0
+        ) + input_raw * jnp.sum(query_vec * key_vec, axis=1, keepdims=True)
         mixed = rms_scale(read, head_gain[...]) * jax.nn.silu(owned(3))
         part = pl.ds(pl.multiple_of(h * dim, dim), dim)
         mx_buf[me, :, part] = mixed.astype(BF16)
 
-    for batch in batches(chips // head_chips):
-        for m in batch:
-            for k in range(m * head_chips, (m + 1) * head_chips):
+    mixed_parts = []
+    for lo, hi in shares:
+        step = max(2, head_chips)
+        for first in range(lo, hi, step):
+            for k in range(first, first + step):
                 for r in range(2):
                     if k or r:
                         moved[k, r].wait_recv()
-        for m in batch:
-            base = flip(chip // head_chips, m)
-            for i in range(chip_heads):
-                head_step(base * chip_heads + i, base * head_chips * 2 + i * per_head)
+            for m in range(first // head_chips, (first + step) // head_chips):
+                base = flip(chip // head_chips, m)
+                for i in range(chip_heads):
+                    head_step(base * chip_heads + i, base * head_chips * 2 + i * per_head)
+        size = (hi - lo) * 2 * cols
+        offset = pl.multiple_of(base_of(chip, lo, hi) * 2 * cols, size)
+        mixed_parts.append(
+            scatter(2 + len(mixed_parts), mx_buf.at[me, :, pl.ds(offset, size)])
+        )
 
     def update_step(h, carry):
         flat = gates[h]
@@ -254,38 +339,49 @@
             )
         return carry
 
-    first_part = heads * 5 // 8
-    second_part = heads * 7 // 8
-
-    copies = spread(2, mx_buf)
+    cuts = [heads * c // 16 for c in (0, 8, 11, 13, 16)]
+
+    def update(c):
+        lax.fori_loop(cuts[c], cuts[c + 1], update_step, 0, unroll=2)
+    passed = {}
+    forward(4, mx_buf, mixed_parts, passed, [0])
     loads[6].wait()
-    lax.fori_loop(0, first_part, update_step, 0, unroll=2)
+    update(0)
+    near = min(1, chips - 1)
+    col_parts = []
 
     def gather_pair(ks):
+        arrive(passed, ks)
         x = jnp.concatenate([part for k in ks for part in chip_rows(mx_buf, k)], axis=0)
         xn[ks[0] * both : (ks[0] + 2) * both, :] = x.astype(BF16)
 
+    def project(lo, hi):
+        acc = jnp.dot(xn[lo * both : hi * both, :], wo[...], preferred_element_type=F32)
+        for k in range(lo, hi):
+            col_buf[me, at[k]] = acc[(k - lo) * both : (k - lo + 1) * both, :].astype(BF16)
+        base = base_of(chip, lo, hi)
+        col_parts.append(
+            scatter(5 + len(col_parts), col_buf.at[me, pl.ds(base, hi - lo)], near, far_first[::-1])
+        )
+
     for j, ks in enumerate(pairs):
-        forward(2, mx_buf, copies, ks)
+        forward(4, mx_buf, mixed_parts, passed, [k for k in ks if k])
         if j:
-            arrive(copies, pairs[j - 1])
             gather_pair(pairs[j - 1])
-    arrive(copies, pairs[-1])
+            ready = 2 * j
+            if ready == chips // 2:
+                project(0, ready)
     gather_pair(pairs[-1])
-
-    acc = jnp.dot(xn[...], wo[...], preferred_element_type=F32)
-    for k in range(chips):
-        col_buf[me, at[k]] = acc[k * both : (k + 1) * both, :].astype(BF16)
-
-    copies = spread(3, col_buf)
-    lax.fori_loop(first_part, second_part, update_step, 0, unroll=2)
+    project(chips // 2, chips)
+    passed = {}
+    forward(6, col_buf, col_parts, passed, [0])
+    update(1)
     loads[7].wait()
     loads[8].wait()
     tile = 256 if hidden % 256 == 0 else hidden
     slab_chips = max(1, 256 // (2 * cols))
     slab = slab_chips * 2 * cols
     slabs = chips // slab_chips
-    plan = batches(slabs)
 
     def slab_of(m):
         base = flip(chip // slab_chips, m)
@@ -299,32 +395,26 @@
         scaled = (middle * norm_ffn[:, part]).reshape(total, slab).astype(BF16)
         return part, scaled, jnp.sum((middle * middle).reshape(total, slab), axis=1, keepdims=True)
 
-    def members(batch):
-        return [k for m in batch for k in range(m * slab_chips, (m + 1) * slab_chips)]
-
-    for b, batch in enumerate(plan):
-        if b == 0:
-            forward(3, col_buf, copies, members(batch))
-        if b + 1 < len(plan) and b > 0:
-            forward(3, col_buf, copies, members(plan[b + 1]))
-        if b == 0 and len(plan) > 1:
-            arrive(copies, members(batch))
-        else:
-            arrive(copies, members(batch))
-        ready = [slab_of(m) for m in batch]
-        power = sum(r[2] for r in ready)
-        if b:
+    following = 1
+    for m in range(slabs):
+        ks = range(m * slab_chips, (m + 1) * slab_chips)
+        ahead = m if m < 2 else min(2 * m, slabs - 1)
+        forward(6, col_buf, col_parts, passed, range(following, (ahead + 1) * slab_chips), near)
+        following = max(following, (ahead + 1) * slab_chips)
+        arrive(passed, ks)
+        part, scaled, power = slab_of(m)
+        if m:
             power = power + squares[...]
-        last = b + 1 == len(plan)
+        last = m + 1 == slabs
         if last:
             scale = lax.rsqrt(power / width + epsilon)
         else:
             squares[...] = power
         for j in range(hidden // tile):
             span = slice(j * tile, (j + 1) * tile)
-            g = sum(jnp.dot(r[1], wg[r[0], span], preferred_element_type=F32) for r in ready)
-            u = sum(jnp.dot(r[1], wu[r[0], span], preferred_element_type=F32) for r in ready)
-            if b:
+            g = jnp.dot(scaled, wg[part, span], preferred_element_type=F32)
+            u = jnp.dot(scaled, wu[part, span], preferred_element_type=F32)
+            if m:
                 g = g + acc_gate[:, span]
                 u = u + acc_up[:, span]
             if last:
@@ -332,25 +422,16 @@
             else:
                 acc_gate[:, span] = g
                 acc_up[:, span] = u
-        if b == 0 and len(plan) > 1:
-            forward(3, col_buf, copies, members(plan[1]))
-
+        if m == 0:
+            update(2)
     loads[9].wait()
     out_tile = 256
     pieces = 4
     piece = width // pieces
 
-    halves = []
-    for p in range(pieces):
-        for q in range(piece // out_tile):
-            part = slice(p * piece + q * out_tile, p * piece + (q + 1) * out_tile)
-            d = jnp.dot(hid[...], wd[:, part], preferred_element_type=F32)
-            for s in range(n):
-                ps[s % 2, s // 2, :, part] = d[s * rows : (s + 1) * rows, :].astype(BF16)
-        part = pl.ds(p * piece, piece)
-        halves.append(send(4, p, ps.at[core, :, :, part], fw.at[:, :, part], partner))
-    returns = []
-    for p in range(pieces):
+    halves, returns = [], []
+
+    def settle(p):
         part = pl.ds(p * piece, piece)
         halves[p].wait_recv()
         for c in range(chips):
@@ -360,14 +441,27 @@
         for k in far_first + [0]:
             returns.append(
                 send(
-                    5 + p,
+                    9 + p,
                     k,
                     summed.at[at[k], :, part],
                     ret_buf.at[chip, :, part],
                     cross[k],
                 )
             )
-    lax.fori_loop(second_part, heads, update_step, 0, unroll=2)
+
+    for p in range(pieces):
+        for q in range(piece // out_tile):
+            part = slice(p * piece + q * out_tile, p * piece + (q + 1) * out_tile)
+            d = jnp.dot(hid[...], wd[:, part], preferred_element_type=F32)
+            for s in range(n):
+                ps[s % 2, s // 2, :, part] = d[s * rows : (s + 1) * rows, :].astype(BF16)
+        part = pl.ds(p * piece, piece)
+        halves.append(send(8, p, ps.at[core, :, :, part], fw.at[:, :, part], partner))
+        if p >= 2:
+            settle(p - 2)
+    for p in range(pieces - 2, pieces):
+        settle(p)
+    update(3)
     for copy in returns:
         copy.wait_recv()
     own = mid_buf[chip]
@@ -385,9 +479,24 @@
             rows_e = rows_e + ret_buf[e * group + s].astype(F32)
         result = result + share * rows_e
     layer_out[...] = result.astype(BF16)
-
     for copy in sent:
         copy.wait_send()
+
+    @pl.when(jnp.logical_not(late))
+    def _():
+        extra.wait_send()
+        for copy in through:
+            copy.wait_send()
+
+
+def write(layer_in, state_in, layer_out, state_out, sem):
+    copies = [pltpu.make_async_copy(layer_in, layer_out, sem.at[0])]
+    for t in range(state_in.shape[0]):
+        copies.append(pltpu.make_async_copy(state_in.at[t], state_out.at[t], sem.at[1 + t]))
+    for copy in copies:
+        copy.start()
+    for copy in copies:
+        copy.wait()
 
 
 def local(n, *args):
@@ -416,7 +525,7 @@
     total = n * rows
     any_spec = pl.BlockSpec(memory_space=pltpu.HBM)
     vmem = pl.BlockSpec(memory_space=pltpu.VMEM)
-    return pl.pallas_call(
+    layer, fresh = pl.pallas_call(
         functools.partial(kernel, n),
         out_shape=(
             pltpu.VMEM(tokens.shape, tokens.dtype),
@@ -451,8 +560,9 @@
             pltpu.VMEM((n // 2, rows, width), BF16),
             pltpu.VMEM((n // 2, rows, width), BF16),
             pltpu.SemaphoreType.DMA((14,)),
-            pltpu.SemaphoreType.DMA((9, n)),
-            pltpu.SemaphoreType.DMA((9, n)),
+            pltpu.SemaphoreType.DMA((13, n)),
+            pltpu.SemaphoreType.DMA((13, n)),
+            pltpu.SemaphoreType.REGULAR,
         ],
         compiler_params=pltpu.CompilerParams(
             collective_id=0,
@@ -476,6 +586,20 @@
         expert_gate,
         expert_up,
         expert_down,
+    )
+    return pl.pallas_call(
+        write,
+        out_shape=(
+            jax.ShapeDtypeStruct(layer.shape, layer.dtype),
+            jax.ShapeDtypeStruct(fresh.shape, fresh.dtype),
+        ),
+        in_specs=[vmem, vmem],
+        out_specs=(any_spec, any_spec),
+        scratch_shapes=[pltpu.SemaphoreType.DMA((1 + rows,))],
+        compiler_params=pltpu.CompilerParams(vmem_limit_bytes=1 << 20),
+    )(
+        pltpu.with_memory_space_constraint(layer, pltpu.VMEM),
+        pltpu.with_memory_space_constraint(fresh, pltpu.VMEM),
     )
 
 

time: 46 us -> 42.9 us (0.933)
  local copies, waits for them, and re-layouts: 2.62 us -> 0 us
    unnamed x2 -> x0, local copies, waits for them, and re-layouts: 2.62 us -> none
    pallas_call x1, Pallas kernels: 42.5 us -> 40 us  [local(): pl.pallas_call(functools.partial(kernel, n), out_shape=(pltpu.VMEM(tokens...]
    pallas_call x0 -> x1, Pallas kernels: none -> 2.06 us  [local(): pl.pallas_call(write, out_shape=(jax.ShapeDtypeStruct(layer.shape, layer....]
where the time goes in v2:
time: 42.9 us; the launch traced here: 42.7 us
  Pallas kernels  42.1 us (98%)
  between operations  0.64 us (1%)
    pallas_call x1, Pallas kernels, local(): pl.pallas_call(functools.partial(kernel, n), out_shape=(pltpu.VMEM(tokens...  40 us
    pallas_call x1, Pallas kernels, local(): pl.pallas_call(write, out_shape=(jax.ShapeDtypeStruct(layer.shape, layer....  2.06 us

profile of v2, /device:TPU:0, one launch (start us, length us, event | category | flops | bytes accessed | tf_op | source)
XLA Modules:
  0.0 42.7 jit_solution(3244812029702119803)
XLA Ops:
  0.6 40.0 %shard_map.167 = (bf16[4,2048]{1,0:T(4,128)(2,1)S(1)}, f32[4,16,128,128]{3,2,1,0:T(8,128)S(1)}) custom-call(bf16[4,2048]{1,0:T(4,128)(2,1)} %tokens.1, f32[4,16,128,128]{3,2,1,0:T(8,128)} %state.1, s32[2,4]{1,0:T(2,128)} %bitcast.9, bf16[2,4]{1,0:T(2,128)(2,1)} %bitcast.10, f32[1,2048]{1,0:T(1,128)} %bitcast.6, bf16[2048,128]{1,0:T(8,128)(2,1)} %w_query.1, ...), custom_call_target="tpu_custom_call" | custom-call | tf_op jit(solution)/shard_map/pallas_call | solution.py:528
  40.6 2.1 %shard_map.168 = (bf16[4,2048]{1,0:T(4,128)(2,1)}, f32[4,16,128,128]{3,2,1,0:T(8,128)}) custom-call(bf16[4,2048]{1,0:T(4,128)(2,1)S(1)} %get-tuple-element.4.layer_in, f32[4,16,128,128]{3,2,1,0:T(8,128)S(1)} %get-tuple-element.5.state_in), custom_call_target="tpu_custom_call" | custom-call | tf_op jit(solution)/shard_map/pallas_call | solution.py:590

commit v3 on v2

--- a/solution.py
+++ b/solution.py
@@ -24,8 +24,8 @@
     n,
     tokens,
     state,
-    ids,
-    weights,
+    ids_in,
+    weights_in,
     norm_mix_in,
     w_query,
     w_forget,
@@ -65,6 +65,8 @@
     fw,
     summed,
     ret_buf,
+    ids,
+    weights,
     load_sem,
     send_sem,
     recv_sem,
@@ -87,6 +89,8 @@
     loads.append(pltpu.make_async_copy(expert_gate, wg, load_sem.at[7]))
     loads.append(pltpu.make_async_copy(expert_up, wu, load_sem.at[8]))
     loads.append(pltpu.make_async_copy(expert_down, wd, load_sem.at[9]))
+    loads.append(pltpu.make_async_copy(ids_in, ids, load_sem.at[14]))
+    loads.append(pltpu.make_async_copy(weights_in, weights, load_sem.at[15]))
     small = [
         pltpu.make_async_copy(a, b, load_sem.at[10 + j])
         for j, (a, b) in enumerate(
@@ -152,44 +156,50 @@
     def _():
         pl.semaphore_wait(barrier, n - 3)
 
-    sent = []
-
-    def handle(phase, slot, source, target, peer):
+    GATHER, MOVE, MIXED, COLUMNS, PAIR, RETURN = range(6)
+
+    def lane(phase, slot, direct):
+        if phase == MOVE or (phase == COLUMNS and not direct):
+            return n + slot
+        if phase == PAIR or (phase == MIXED and direct):
+            return 2 * n + slot
+        return 2 * n + chips if phase == RETURN else slot
+
+    def handle(phase, slot, source, target, peer, direct=False):
         return pltpu.make_async_remote_copy(
             src_ref=source,
             dst_ref=target,
-            send_sem=send_sem.at[phase, slot],
-            recv_sem=recv_sem.at[phase, slot],
+            send_sem=send_sem.at[phase],
+            recv_sem=recv_sem.at[lane(phase, slot, direct)],
             device_id={"ep": peer},
             device_id_type=pl.DeviceIdType.MESH,
         )
 
-    def send(phase, slot, source, target, peer):
-        copy = handle(phase, slot, source, target, peer)
+    def send(phase, slot, source, target, peer, direct=False):
+        copy = handle(phase, slot, source, target, peer, direct)
         copy.start()
-        sent.append(copy)
         return copy
 
-    def scatter(phase, block, near=0, order=None):
-        return {
-            k: (
-                [send(phase, k, block, block, cross[k])]
-                + ([send(phase, chips + k, block, block, same[k])] if k <= near else [])
-            )
-            for k in order or far_first
-        }
-
-    def forward(phase, buf, copies, passed, ks, near=0):
+    def whole(phase, slot, block, direct=False):
+        return handle(phase, slot, block, block, partner, direct)
+
+    def scatter(phase, block, near=0):
+        for k in far_first:
+            send(phase, k, block, block, cross[k], True)
+            if k <= near:
+                send(phase, chips + k, block, block, same[k])
+
+    def forward(phase, buf, passed, ks, near=0):
         for k in ks:
-            for part in copies:
-                if k:
-                    for copy in part[k]:
-                        copy.wait_recv()
             if k == 0:
                 passed[k] = send(phase, 0, buf.at[me], buf.at[me], partner)
-            elif k > near:
+            else:
                 block = buf.at[cross[k]]
-                passed[k] = send(phase, chips + k, block, block, partner)
+                whole(phase, k, block, True).wait_recv()
+                if k > near:
+                    passed[k] = send(phase, chips + k, block, block, partner)
+                else:
+                    whole(phase, chips + k, buf.at[same[k]]).wait_recv()
 
     def arrive(passed, ks):
         for k in ks:
@@ -210,8 +220,8 @@
     extra = pltpu.make_async_remote_copy(
         src_ref=own,
         dst_ref=own,
-        send_sem=send_sem.at[7, 0],
-        recv_sem=recv_sem.at[0, chips + to_late],
+        send_sem=send_sem.at[GATHER],
+        recv_sem=recv_sem.at[chips + to_late],
         device_id={"ep": n - 2 + core},
         device_id_type=pl.DeviceIdType.MESH,
     )
@@ -228,7 +238,6 @@
         extra.start()
 
     handle(0, to_late, own, own, n - 1 - core).start()
-    sent.extend(direct)
     through = []
 
     for load in small:
@@ -273,7 +282,7 @@
         for r, peer in enumerate((same[k], cross[k])):
             if k or r:
                 source = pj_send.at[2 * k + (core if r == 0 else 1 - core)]
-                moved[k, r] = send(1, 2 * k + r, source, pj_buf.at[me], peer)
+                moved[k, r] = send(MOVE, 2 * k + r, source, pj_buf.at[me], peer)
     pj_buf[me] = pj_send[core]
     per_head = max(1, dim // cols)
     head_chips = max(1, per_head // 2)
@@ -310,7 +319,6 @@
         part = pl.ds(pl.multiple_of(h * dim, dim), dim)
         mx_buf[me, :, part] = mixed.astype(BF16)
 
-    mixed_parts = []
     for lo, hi in shares:
         step = max(2, head_chips)
         for first in range(lo, hi, step):
@@ -324,9 +332,7 @@
                     head_step(base * chip_heads + i, base * head_chips * 2 + i * per_head)
         size = (hi - lo) * 2 * cols
         offset = pl.multiple_of(base_of(chip, lo, hi) * 2 * cols, size)
-        mixed_parts.append(
-            scatter(2 + len(mixed_parts), mx_buf.at[me, :, pl.ds(offset, size)])
-        )
+        scatter(MIXED, mx_buf.at[me, :, pl.ds(offset, size)])
 
     def update_step(h, carry):
         flat = gates[h]
@@ -344,11 +350,10 @@
     def update(c):
         lax.fori_loop(cuts[c], cuts[c + 1], update_step, 0, unroll=2)
     passed = {}
-    forward(4, mx_buf, mixed_parts, passed, [0])
+    forward(MIXED, mx_buf, passed, [0])
     loads[6].wait()
     update(0)
     near = min(1, chips - 1)
-    col_parts = []
 
     def gather_pair(ks):
         arrive(passed, ks)
@@ -360,12 +365,10 @@
         for k in range(lo, hi):
             col_buf[me, at[k]] = acc[(k - lo) * both : (k - lo + 1) * both, :].astype(BF16)
         base = base_of(chip, lo, hi)
-        col_parts.append(
-            scatter(5 + len(col_parts), col_buf.at[me, pl.ds(base, hi - lo)], near, far_first[::-1])
-        )
+        scatter(COLUMNS, col_buf.at[me, pl.ds(base, hi - lo)], near)
 
     for j, ks in enumerate(pairs):
-        forward(4, mx_buf, mixed_parts, passed, [k for k in ks if k])
+        forward(MIXED, mx_buf, passed, [k for k in ks if k])
         if j:
             gather_pair(pairs[j - 1])
             ready = 2 * j
@@ -374,7 +377,7 @@
     gather_pair(pairs[-1])
     project(chips // 2, chips)
     passed = {}
-    forward(6, col_buf, col_parts, passed, [0])
+    forward(COLUMNS, col_buf, passed, [0])
     update(1)
     loads[7].wait()
     loads[8].wait()
@@ -383,37 +386,53 @@
     slab = slab_chips * 2 * cols
     slabs = chips // slab_chips
 
-    def slab_of(m):
-        base = flip(chip // slab_chips, m)
-        first = base * slab_chips * 2
-        part = pl.ds(pl.multiple_of(base * slab, slab), slab)
-        y = jnp.concatenate(
-            [col_buf[first + i].astype(F32) for i in range(2 * slab_chips)], axis=2
-        )
+    def piece_of(first, count, offset, size):
+        part = pl.ds(pl.multiple_of(offset, size), size)
+        y = jnp.concatenate([col_buf[first + i].astype(F32) for i in range(count)], axis=2)
         middle = mid_buf[:, :, part] + y
         mid_buf[:, :, part] = middle
-        scaled = (middle * norm_ffn[:, part]).reshape(total, slab).astype(BF16)
-        return part, scaled, jnp.sum((middle * middle).reshape(total, slab), axis=1, keepdims=True)
-
-    following = 1
-    for m in range(slabs):
-        ks = range(m * slab_chips, (m + 1) * slab_chips)
-        ahead = m if m < 2 else min(2 * m, slabs - 1)
-        forward(6, col_buf, col_parts, passed, range(following, (ahead + 1) * slab_chips), near)
-        following = max(following, (ahead + 1) * slab_chips)
-        arrive(passed, ks)
-        part, scaled, power = slab_of(m)
+        scaled = (middle * norm_ffn[:, part]).reshape(total, size).astype(BF16)
+        return part, scaled, jnp.sum((middle * middle).reshape(total, size), axis=1, keepdims=True)
+
+    steps = []
+    if cols % 128 == 0:
+
+        def devices(peers):
+            return [(peer, 1, peer * cols, cols) for peer in peers]
+
+        steps.append(([], [0], [(2 * chip, 2, chip * slab, slab)]))
+        if near:
+            steps.append(([1], [], [(2 * at[1], 2, at[1] * slab, slab)]))
+        rest = [[k, k + 1] for k in range(2 * near, chips, 2)]
+        for ks in rest:
+            steps.append((ks, [], devices(cross[k] for k in ks)))
+        for ks in rest:
+            steps.append(([], ks, devices(same[k] for k in ks)))
+    else:
+        for m in range(slabs):
+            ks = list(range(m * slab_chips, (m + 1) * slab_chips))
+            base = flip(chip // slab_chips, m)
+            steps.append((ks[m == 0 :], ks, [(base * slab_chips * 2, 2 * slab_chips, base * slab, slab)]))
+
+    for m, (coming, there, pieces) in enumerate(steps):
+        forward(COLUMNS, col_buf, passed, coming, near)
+        arrive(passed, there)
+        ready = [piece_of(*piece) for piece in pieces]
+        power = sum(piece[2] for piece in ready)
+        scaled = jnp.concatenate([piece[1] for piece in ready], axis=1)
         if m:
             power = power + squares[...]
-        last = m + 1 == slabs
+        last = m + 1 == len(steps)
         if last:
             scale = lax.rsqrt(power / width + epsilon)
         else:
             squares[...] = power
         for j in range(hidden // tile):
             span = slice(j * tile, (j + 1) * tile)
-            g = jnp.dot(scaled, wg[part, span], preferred_element_type=F32)
-            u = jnp.dot(scaled, wu[part, span], preferred_element_type=F32)
+            g_rows = jnp.concatenate([wg[piece[0], span] for piece in ready], axis=0)
+            u_rows = jnp.concatenate([wu[piece[0], span] for piece in ready], axis=0)
+            g = jnp.dot(scaled, g_rows, preferred_element_type=F32)
+            u = jnp.dot(scaled, u_rows, preferred_element_type=F32)
             if m:
                 g = g + acc_gate[:, span]
                 u = u + acc_up[:, span]
@@ -426,44 +445,50 @@
             update(2)
     loads[9].wait()
     out_tile = 256
-    pieces = 4
-    piece = width // pieces
-
-    halves, returns = [], []
+    counts = [2]*(width//(2*out_tile))
+    bounds = [sum(counts[:p]) * out_tile for p in range(len(counts) + 1)]
+
+    halves = []
 
     def settle(p):
-        part = pl.ds(p * piece, piece)
+        part = pl.ds(bounds[p], bounds[p + 1] - bounds[p])
         halves[p].wait_recv()
         for c in range(chips):
             summed[c, :, part] = (
                 ps[1 - core, c, :, part].astype(F32) + fw[c, :, part].astype(F32)
             ).astype(BF16)
         for k in far_first + [0]:
-            returns.append(
-                send(
-                    9 + p,
-                    k,
-                    summed.at[at[k], :, part],
-                    ret_buf.at[chip, :, part],
-                    cross[k],
-                )
+            send(
+                RETURN, k, summed.at[at[k], :, part], ret_buf.at[chip, :, part], cross[k]
             )
 
-    for p in range(pieces):
-        for q in range(piece // out_tile):
-            part = slice(p * piece + q * out_tile, p * piece + (q + 1) * out_tile)
+    for p in range(len(counts)):
+        for q in range(counts[p]):
+            part = slice(bounds[p] + q * out_tile, bounds[p] + (q + 1) * out_tile)
             d = jnp.dot(hid[...], wd[:, part], preferred_element_type=F32)
             for s in range(n):
                 ps[s % 2, s // 2, :, part] = d[s * rows : (s + 1) * rows, :].astype(BF16)
-        part = pl.ds(p * piece, piece)
-        halves.append(send(8, p, ps.at[core, :, :, part], fw.at[:, :, part], partner))
+        part = pl.ds(bounds[p], bounds[p + 1] - bounds[p])
+        halves.append(send(PAIR, p, ps.at[core, :, :, part], fw.at[:, :, part], partner))
         if p >= 2:
             settle(p - 2)
-    for p in range(pieces - 2, pieces):
+    for p in range(len(counts) - 2, len(counts)):
         settle(p)
     update(3)
-    for copy in returns:
-        copy.wait_recv()
+    for phase, buf in ((MOVE, pj_send), (MIXED, mx_buf), (COLUMNS, col_buf)):
+        whole(phase, 0, buf.at[pl.ds(0, n - 1)]).wait_send()
+    whole(PAIR, 0, ps.at[0]).wait_send()
+
+    @pl.when(late)
+    def _():
+        whole(GATHER, 0, tok_buf.at[pl.ds(0, chips)]).wait_send()
+
+    @pl.when(jnp.logical_not(late))
+    def _():
+        whole(GATHER, 0, tok_buf).wait_send()
+    whole(RETURN, 0, ret_buf).wait_recv()
+    for load in loads[10:]:
+        load.wait()
     own = mid_buf[chip]
     result = jnp.where(core == 0, own[:rows, :], own[rows:, :])
     diagonal = lax.broadcasted_iota(jnp.int32, (rows, rows), 0) == lax.broadcasted_iota(
@@ -479,14 +504,7 @@
             rows_e = rows_e + ret_buf[e * group + s].astype(F32)
         result = result + share * rows_e
     layer_out[...] = result.astype(BF16)
-    for copy in sent:
-        copy.wait_send()
-
-    @pl.when(jnp.logical_not(late))
-    def _():
-        extra.wait_send()
-        for copy in through:
-            copy.wait_send()
+    whole(RETURN, 0, summed).wait_send()
 
 
 def write(layer_in, state_in, layer_out, state_out, sem):
@@ -531,7 +549,7 @@
             pltpu.VMEM(tokens.shape, tokens.dtype),
             pltpu.VMEM(state.shape, state.dtype),
         ),
-        in_specs=[any_spec, any_spec, vmem, vmem] + [any_spec] * 12,
+        in_specs=[any_spec] * 16,
         out_specs=(vmem, vmem),
         scratch_shapes=[
             pltpu.VMEM((n, rows, width), BF16),
@@ -559,9 +577,11 @@
             pltpu.VMEM((n // 2, rows, width), BF16),
             pltpu.VMEM((n // 2, rows, width), BF16),
             pltpu.VMEM((n // 2, rows, width), BF16),
-            pltpu.SemaphoreType.DMA((14,)),
-            pltpu.SemaphoreType.DMA((13, n)),
-            pltpu.SemaphoreType.DMA((13, n)),
+            pltpu.VMEM(ids.T.shape, ids.dtype),
+            pltpu.VMEM(weights.T.shape, weights.dtype),
+            pltpu.SemaphoreType.DMA((16,)),
+            pltpu.SemaphoreType.DMA((6,)),
+            pltpu.SemaphoreType.DMA((2 * n + n // 2 + 1,)),
             pltpu.SemaphoreType.REGULAR,
         ],
         compiler_params=pltpu.CompilerParams(

time: 42.9 us -> 38.7 us (0.902)
  Pallas kernels: 42.1 us -> 37.9 us
    pallas_call x1, Pallas kernels: 40 us -> 35.8 us  [local(): pl.pallas_call(functools.partial(kernel, n), out_shape=(pltpu.VMEM(tokens...]
where the time goes in v3:
time: 38.7 us; the launch traced here: 38.5 us
  Pallas kernels  37.9 us (98%)
  between operations  0.64 us (2%)
    pallas_call x1, Pallas kernels, local(): pl.pallas_call(functools.partial(kernel, n), out_shape=(pltpu.VMEM(tokens...  35.8 us
    pallas_call x1, Pallas kernels, local(): pl.pallas_call(write, out_shape=(jax.ShapeDtypeStruct(layer.shape, layer....  2.06 us

profile of v3, /device:TPU:0, one launch (start us, length us, event | category | flops | bytes accessed | tf_op | source)
XLA Modules:
  0.0 38.5 jit_solution(2338135795285650499)
XLA Ops:
  0.6 35.8 %shard_map.167 = (bf16[4,2048]{1,0:T(4,128)(2,1)S(1)}, f32[4,16,128,128]{3,2,1,0:T(8,128)S(1)}) custom-call(bf16[4,2048]{1,0:T(4,128)(2,1)} %tokens.1, f32[4,16,128,128]{3,2,1,0:T(8,128)} %state.1, s32[2,4]{1,0:T(2,128)} %bitcast.9, bf16[2,4]{1,0:T(2,128)(2,1)} %bitcast.10, f32[1,2048]{1,0:T(1,128)} %bitcast.6, bf16[2048,128]{1,0:T(8,128)(2,1)} %w_query.1, ...), custom_call_target="tpu_custom_call" | custom-call | tf_op jit(solution)/shard_map/pallas_call | solution.py:546
  36.5 2.1 %shard_map.168 = (bf16[4,2048]{1,0:T(4,128)(2,1)}, f32[4,16,128,128]{3,2,1,0:T(8,128)}) custom-call(bf16[4,2048]{1,0:T(4,128)(2,1)S(1)} %get-tuple-element.4.layer_in, f32[4,16,128,128]{3,2,1,0:T(8,128)S(1)} %get-tuple-element.5.state_in), custom_call_target="tpu_custom_call" | custom-call | tf_op jit(solution)/shard_map/pallas_call | solution.py:610

commit v4 on v3

--- a/solution.py
+++ b/solution.py
@@ -158,12 +158,20 @@
 
     GATHER, MOVE, MIXED, COLUMNS, PAIR, RETURN = range(6)
 
+    second, third = chips + chips // 2, 2 * chips + 1
+
     def lane(phase, slot, direct):
-        if phase == MOVE or (phase == COLUMNS and not direct):
-            return n + slot
-        if phase == PAIR or (phase == MIXED and direct):
-            return 2 * n + slot
-        return 2 * n + chips if phase == RETURN else slot
+        if phase == MOVE:
+            return second + slot // 4
+        if phase == PAIR or (phase == MIXED and direct and slot):
+            return third + slot
+        if phase == RETURN:
+            return third + chips
+        if phase == COLUMNS and not direct:
+            if slot == chips + 1:
+                return second + chips // 2
+            return second + (slot - chips) // 2 if slot else second
+        return slot if direct else chips + (slot - chips) // 2
 
     def handle(phase, slot, source, target, peer, direct=False):
         return pltpu.make_async_remote_copy(
@@ -189,24 +197,28 @@
             if k <= near:
                 send(phase, chips + k, block, block, same[k])
 
-    def forward(phase, buf, passed, ks, near=0):
+    def forward(phase, buf, ks, near=0):
         for k in ks:
             if k == 0:
-                passed[k] = send(phase, 0, buf.at[me], buf.at[me], partner)
+                send(phase, 0, buf.at[me], buf.at[me], partner, phase != COLUMNS)
             else:
                 block = buf.at[cross[k]]
                 whole(phase, k, block, True).wait_recv()
                 if k > near:
-                    passed[k] = send(phase, chips + k, block, block, partner)
+                    send(phase, chips + k, block, block, partner)
                 else:
                     whole(phase, chips + k, buf.at[same[k]]).wait_recv()
 
-    def arrive(passed, ks):
-        for k in ks:
-            if k in passed:
-                passed[k].wait_recv()
-
-    shares = [(0, chips // 2), (chips // 2, chips * 3 // 4), (chips * 3 // 4, chips)]
+    def arrive(phase, buf, ks, near=0):
+        for k in ks[::2]:
+            if k:
+                whole(phase, chips + k, buf.at[pl.ds(0, 2)]).wait_recv()
+            else:
+                whole(phase, 0, buf.at[0], phase != COLUMNS).wait_recv()
+                if near < 1:
+                    whole(phase, chips + 1, buf.at[0]).wait_recv()
+
+    shares = [(chips * i // 4, chips * (i + 1) // 4) for i in range(4)]
 
     def base_of(index, lo, hi):
         return flip(index // (hi - lo), lo // (hi - lo)) * (hi - lo)
@@ -216,12 +228,12 @@
     loads[0].wait()
     own = tok_buf.at[me]
     to_late = sum(bit * (1 - lax.rem(chip // bit, 2)) for bit in bits)
-    direct = [handle(0, k, own, own, cross[k] if k else partner) for k in range(chips)]
+    direct = [handle(GATHER, k, own, own, cross[k] if k else partner, True) for k in range(chips)]
     extra = pltpu.make_async_remote_copy(
         src_ref=own,
         dst_ref=own,
         send_sem=send_sem.at[GATHER],
-        recv_sem=recv_sem.at[chips + to_late],
+        recv_sem=recv_sem.at[chips + to_late // 2],
         device_id={"ep": n - 2 + core},
         device_id_type=pl.DeviceIdType.MESH,
     )
@@ -237,53 +249,61 @@
         pl.semaphore_wait(late_sem, 2)
         extra.start()
 
-    handle(0, to_late, own, own, n - 1 - core).start()
-    through = []
+    handle(GATHER, to_late, own, own, n - 1 - core, True).start()
 
     for load in small:
         load.wait()
     pairs = [[2 * j, 2 * j + 1] for j in range(chips // 2)]
 
-    def norm_pair(ks):
-        x = jnp.concatenate([part for k in ks for part in chip_rows(tok_buf, k)], axis=0)
-        for i, k in enumerate(ks):
-            mid_buf[at[k]] = x[i * both : (i + 1) * both, :]
-        xn[ks[0] * both : (ks[0] + 2) * both, :] = rms_scale(x, norm_mix[...]).astype(BF16)
-
-    def pass_on(k):
-        direct[k].wait_recv()
-        block = tok_buf.at[cross[k]]
-        through.append(handle(0, chips + k, block, block, partner))
+    def norm_pair(j):
+        x = jnp.concatenate([tok_buf[4 * j + i].astype(F32) for i in range(4)], axis=0)
+        for i in range(2):
+            mid_buf[2 * j + i] = x[i * both : (i + 1) * both, :]
+        span = pl.ds(pl.multiple_of(2 * j * both, 2 * both), 2 * both)
+        xn[span, :] = rms_scale(x, norm_mix[...]).astype(BF16)
+
+    def relation(index):
+        return sum(bit * lax.rem(chip // bit + index // bit, 2) for bit in bits)
+
+    def pass_on(index):
+        slot = relation(index)
+        whole(GATHER, slot, own, True).wait_recv()
 
         @pl.when(jnp.logical_not(late))
         def _():
-            through[-1].start()
-
-    def settle_pair(ks):
-        for k in ks:
-            (through[k - 1] if k else direct[0]).wait_recv()
-        norm_pair(ks)
-
-    for j, ks in enumerate(pairs):
-        for k in ks:
-            if k:
-                pass_on(k)
-        if j:
-            settle_pair(pairs[j - 1])
-    settle_pair(pairs[-1])
+            block = tok_buf.at[2 * index + 1 - core]
+            send(GATHER, chips + slot, block, block, partner)
+
+    def settle_pair(j, first):
+        if first:
+            whole(GATHER, chips + 1, own).wait_recv()
+        else:
+            whole(GATHER, chips + relation(2 * j), tok_buf.at[pl.ds(0, 2)]).wait_recv()
+        norm_pair(j)
+
+    plane, planes = chip // 2, chips // 2
+    order = [plane]
+    for i in range(planes - 1):
+        above = (i < planes - 1 - plane).astype(jnp.int32)
+        order.append(above * (plane + 1 + i) + (1 - above) * (planes - 2 - i))
+    whole(GATHER, 0, own, True).wait_recv()
+    pass_on(at[1])
+    for i in range(1, planes):
+        pass_on(2 * order[i])
+        pass_on(2 * order[i] + 1)
+        settle_pair(order[i - 1], i == 1)
+    settle_pair(order[-1], planes == 1)
     for load in loads[1:5]:
         load.wait()
     w_all = jnp.concatenate([wp[j] for j in range(4)], axis=1)
     acc = jnp.dot(xn[...], w_all, preferred_element_type=F32)
     for s in range(n):
         pj_send[s] = acc[s * rows : (s + 1) * rows, :].astype(BF16)
-    moved = {}
     for k in far_first + [0]:
         for r, peer in enumerate((same[k], cross[k])):
             if k or r:
-                source = pj_send.at[2 * k + (core if r == 0 else 1 - core)]
-                moved[k, r] = send(MOVE, 2 * k + r, source, pj_buf.at[me], peer)
-    pj_buf[me] = pj_send[core]
+                send(MOVE, 2 * k + r, pj_send.at[peer], pj_buf.at[me], peer)
+    pj_buf[me] = pj_send[me]
     per_head = max(1, dim // cols)
     head_chips = max(1, per_head // 2)
     chip_heads = head_chips * 2 * cols // dim
@@ -322,10 +342,9 @@
     for lo, hi in shares:
         step = max(2, head_chips)
         for first in range(lo, hi, step):
-            for k in range(first, first + step):
-                for r in range(2):
-                    if k or r:
-                        moved[k, r].wait_recv()
+            for k in range(first, first + step, 2):
+                count = 4 if k else 3
+                whole(MOVE, 2 * k, pj_buf.at[pl.ds(0, count)]).wait_recv()
             for m in range(first // head_chips, (first + step) // head_chips):
                 base = flip(chip // head_chips, m)
                 for i in range(chip_heads):
@@ -349,14 +368,13 @@
 
     def update(c):
         lax.fori_loop(cuts[c], cuts[c + 1], update_step, 0, unroll=2)
-    passed = {}
-    forward(MIXED, mx_buf, passed, [0])
+    forward(MIXED, mx_buf, [0])
     loads[6].wait()
     update(0)
     near = min(1, chips - 1)
 
     def gather_pair(ks):
-        arrive(passed, ks)
+        arrive(MIXED, mx_buf, ks)
         x = jnp.concatenate([part for k in ks for part in chip_rows(mx_buf, k)], axis=0)
         xn[ks[0] * both : (ks[0] + 2) * both, :] = x.astype(BF16)
 
@@ -368,16 +386,17 @@
         scatter(COLUMNS, col_buf.at[me, pl.ds(base, hi - lo)], near)
 
     for j, ks in enumerate(pairs):
-        forward(MIXED, mx_buf, passed, [k for k in ks if k])
+        forward(MIXED, mx_buf, [k for k in ks if k])
         if j:
             gather_pair(pairs[j - 1])
             ready = 2 * j
+            if ready == chips // 4:
+                project(0, ready)
             if ready == chips // 2:
-                project(0, ready)
+                project(chips // 4, ready)
     gather_pair(pairs[-1])
     project(chips // 2, chips)
-    passed = {}
-    forward(COLUMNS, col_buf, passed, [0])
+    forward(COLUMNS, col_buf, [0])
     update(1)
     loads[7].wait()
     loads[8].wait()
@@ -415,8 +434,8 @@
             steps.append((ks[m == 0 :], ks, [(base * slab_chips * 2, 2 * slab_chips, base * slab, slab)]))
 
     for m, (coming, there, pieces) in enumerate(steps):
-        forward(COLUMNS, col_buf, passed, coming, near)
-        arrive(passed, there)
+        forward(COLUMNS, col_buf, coming, near)
+        arrive(COLUMNS, col_buf, there, near)
         ready = [piece_of(*piece) for piece in pieces]
         power = sum(piece[2] for piece in ready)
         scaled = jnp.concatenate([piece[1] for piece in ready], axis=1)
@@ -581,7 +600,7 @@
             pltpu.VMEM(weights.T.shape, weights.dtype),
             pltpu.SemaphoreType.DMA((16,)),
             pltpu.SemaphoreType.DMA((6,)),
-            pltpu.SemaphoreType.DMA((2 * n + n // 2 + 1,)),
+            pltpu.SemaphoreType.DMA((3 * (n // 2) + 2,)),
             pltpu.SemaphoreType.REGULAR,
         ],
         compiler_params=pltpu.CompilerParams(

time: 38.7 us -> 37.9 us (0.979)
  Pallas kernels: 37.9 us -> 37.1 us
    pallas_call x1, Pallas kernels: 35.8 us -> 35 us  [local(): pl.pallas_call(functools.partial(kernel, n), out_shape=(pltpu.VMEM(tokens...]
where the time goes in v4:
time: 37.9 us; the launch traced here: 37.7 us
  Pallas kernels  37.1 us (98%)
  between operations  0.64 us (2%)
    pallas_call x1, Pallas kernels, local(): pl.pallas_call(functools.partial(kernel, n), out_shape=(pltpu.VMEM(tokens...  35 us
    pallas_call x1, Pallas kernels, local(): pl.pallas_call(write, out_shape=(jax.ShapeDtypeStruct(layer.shape, layer....  2.06 us

profile of v4, /device:TPU:0, one launch (start us, length us, event | category | flops | bytes accessed | tf_op | source)
XLA Modules:
  0.0 37.7 jit_solution(5380466975490917627)
XLA Ops:
  0.6 35.0 %shard_map.167 = (bf16[4,2048]{1,0:T(4,128)(2,1)S(1)}, f32[4,16,128,128]{3,2,1,0:T(8,128)S(1)}) custom-call(bf16[4,2048]{1,0:T(4,128)(2,1)} %tokens.1, f32[4,16,128,128]{3,2,1,0:T(8,128)} %state.1, s32[2,4]{1,0:T(2,128)} %bitcast.9, bf16[2,4]{1,0:T(2,128)(2,1)} %bitcast.10, f32[1,2048]{1,0:T(1,128)} %bitcast.6, bf16[2048,128]{1,0:T(8,128)(2,1)} %w_query.1, ...), custom_call_target="tpu_custom_call" | custom-call | tf_op jit(solution)/shard_map/pallas_call | solution.py:565
  35.7 2.1 %shard_map.168 = (bf16[4,2048]{1,0:T(4,128)(2,1)}, f32[4,16,128,128]{3,2,1,0:T(8,128)}) custom-call(bf16[4,2048]{1,0:T(4,128)(2,1)S(1)} %get-tuple-element.4.layer_in, f32[4,16,128,128]{3,2,1,0:T(8,128)S(1)} %get-tuple-element.5.state_in), custom_call_target="tpu_custom_call" | custom-call | tf_op jit(solution)/shard_map/pallas_call | solution.py:629

commit v5 on v4

--- a/solution.py
+++ b/solution.py
@@ -149,11 +149,13 @@
             signal(late_sem, same[k])
             signal(late_sem, cross[k])
 
-    for load in small + loads[1:]:
+    for load in small:
         load.start()
 
     @pl.when(jnp.logical_not(late))
     def _():
+        for load in loads[1:]:
+            load.start()
         pl.semaphore_wait(barrier, n - 3)
 
     GATHER, MOVE, MIXED, COLUMNS, PAIR, RETURN = range(6)
@@ -218,7 +220,7 @@
                 if near < 1:
                     whole(phase, chips + 1, buf.at[0]).wait_recv()
 
-    shares = [(chips * i // 4, chips * (i + 1) // 4) for i in range(4)]
+    shares = [(0, chips // 4), (chips // 4, chips // 2), (chips // 2, chips)]
 
     def base_of(index, lo, hi):
         return flip(index // (hi - lo), lo // (hi - lo)) * (hi - lo)
@@ -250,6 +252,11 @@
         extra.start()
 
     handle(GATHER, to_late, own, own, n - 1 - core, True).start()
+
+    @pl.when(late)
+    def _():
+        for load in loads[1:]:
+            load.start()
 
     for load in small:
         load.wait()
@@ -340,7 +347,7 @@
         mx_buf[me, :, part] = mixed.astype(BF16)
 
     for lo, hi in shares:
-        step = max(2, head_chips)
+        step = max(2, head_chips, hi - lo)
         for first in range(lo, hi, step):
             for k in range(first, first + step, 2):
                 count = 4 if k else 3

time: 37.9 us -> 37.9 us (level)
  no operation moved by 1% of the time
where the time goes in v5:
time: 37.9 us; the launch traced here: 37.7 us
  Pallas kernels  37.1 us (98%)
  between operations  0.64 us (2%)
    pallas_call x1, Pallas kernels, local(): pl.pallas_call(functools.partial(kernel, n), out_shape=(pltpu.VMEM(tokens...  35 us
    pallas_call x1, Pallas kernels, local(): pl.pallas_call(write, out_shape=(jax.ShapeDtypeStruct(layer.shape, layer....  2.06 us

profile of v5, /device:TPU:0, one launch (start us, length us, event | category | flops | bytes accessed | tf_op | source)
XLA Modules:
  0.0 37.7 jit_solution(13348568173156634125)
XLA Ops:
  0.6 35.0 %shard_map.167 = (bf16[4,2048]{1,0:T(4,128)(2,1)S(1)}, f32[4,16,128,128]{3,2,1,0:T(8,128)S(1)}) custom-call(bf16[4,2048]{1,0:T(4,128)(2,1)} %tokens.1, f32[4,16,128,128]{3,2,1,0:T(8,128)} %state.1, s32[2,4]{1,0:T(2,128)} %bitcast.9, bf16[2,4]{1,0:T(2,128)(2,1)} %bitcast.10, f32[1,2048]{1,0:T(1,128)} %bitcast.6, bf16[2048,128]{1,0:T(8,128)(2,1)} %w_query.1, ...), custom_call_target="tpu_custom_call" | custom-call | tf_op jit(solution)/shard_map/pallas_call | solution.py:572
  35.7 2.1 %shard_map.168 = (bf16[4,2048]{1,0:T(4,128)(2,1)}, f32[4,16,128,128]{3,2,1,0:T(8,128)}) custom-call(bf16[4,2048]{1,0:T(4,128)(2,1)S(1)} %get-tuple-element.4.layer_in, f32[4,16,128,128]{3,2,1,0:T(8,128)S(1)} %get-tuple-element.5.state_in), custom_call_target="tpu_custom_call" | custom-call | tf_op jit(solution)/shard_map/pallas_call | solution.py:636

commit v6 on v4

--- a/solution.py
+++ b/solution.py
@@ -464,7 +464,7 @@
             update(2)
     loads[9].wait()
     out_tile = 256
-    counts = [2]*(width//(2*out_tile))
+    counts = [1] + [2] * (width // (2 * out_tile) - 2) + [3]
     bounds = [sum(counts[:p]) * out_tile for p in range(len(counts) + 1)]
 
     halves = []

time: 37.9 us -> 38 us (level)
  no operation moved by 1% of the time
where the time goes in v6:
time: 38 us; the launch traced here: 37.8 us
  Pallas kernels  37.2 us (98%)
  between operations  0.64 us (2%)
    pallas_call x1, Pallas kernels, local(): pl.pallas_call(functools.partial(kernel, n), out_shape=(pltpu.VMEM(tokens...  35.1 us
    pallas_call x1, Pallas kernels, local(): pl.pallas_call(write, out_shape=(jax.ShapeDtypeStruct(layer.shape, layer....  2.06 us

profile of v6, /device:TPU:0, one launch (start us, length us, event | category | flops | bytes accessed | tf_op | source)
XLA Modules:
  0.0 37.8 jit_solution(13573004460981819714)
XLA Ops:
  0.6 35.1 %shard_map.167 = (bf16[4,2048]{1,0:T(4,128)(2,1)S(1)}, f32[4,16,128,128]{3,2,1,0:T(8,128)S(1)}) custom-call(bf16[4,2048]{1,0:T(4,128)(2,1)} %tokens.1, f32[4,16,128,128]{3,2,1,0:T(8,128)} %state.1, s32[2,4]{1,0:T(2,128)} %bitcast.9, bf16[2,4]{1,0:T(2,128)(2,1)} %bitcast.10, f32[1,2048]{1,0:T(1,128)} %bitcast.6, bf16[2048,128]{1,0:T(8,128)(2,1)} %w_query.1, ...), custom_call_target="tpu_custom_call" | custom-call | tf_op jit(solution)/shard_map/pallas_call | solution.py:565
  35.8 2.1 %shard_map.168 = (bf16[4,2048]{1,0:T(4,128)(2,1)}, f32[4,16,128,128]{3,2,1,0:T(8,128)}) custom-call(bf16[4,2048]{1,0:T(4,128)(2,1)S(1)} %get-tuple-element.4.layer_in, f32[4,16,128,128]{3,2,1,0:T(8,128)S(1)} %get-tuple-element.5.state_in), custom_call_target="tpu_custom_call" | custom-call | tf_op jit(solution)/shard_map/pallas_call | solution.py:629
